TPU v7x, 32 devices: a whole 2x2x4 slice. The times are simulated.
32 devices in a mesh: grp: 2 (over y), sp: 4 (over z), tp: 4 (over x, core).
Axes of the slice: x: 2, y: 2, z: 4, core: 2. Of those that a mesh axis runs over, the one named last changes fastest.
Arguments:
- conv_input: bfloat16 [4096, 1024], P(('grp', 'sp'), 'tp'), parts along dimension 0, may hold values from -6 to 6
- pre_gate: bfloat16 [4096, 1024], P(('grp', 'sp'), 'tp'), parts along dimension 0, may hold values from -6 to 6
- post_gate: bfloat16 [4096, 1024], P(('grp', 'sp'), 'tp'), parts along dimension 0, may hold values from -6 to 6
- conv_taps: float32 [3, 1024], replicated, may hold values from -3.5 to 3.5
- out_proj: bfloat16 [1024, 2048], replicated, may hold values from -0.1875 to 0.1875
- residual_in: bfloat16 [4096, 2048], P(('grp', 'sp', 'tp')), parts along dimension 0, may hold values from -6 to 6
- norm_gain: float32 [2048], replicated, may hold values from 0.1 to 1.9
- routes: int32 [4096, 2], P(('grp', 'sp', 'tp')), parts along dimension 0, may hold values from 0 to 7, as said below
- route_weight: float32 [4096, 2], P(('grp', 'sp', 'tp')), parts along dimension 0, may hold values from 0.1 to 1
- w_gate: bfloat16 [8, 2048, 1024], P('sp', None, 'tp'), may hold values from -0.125 to 0.125
- w_up: bfloat16 [8, 2048, 1024], P('sp', None, 'tp'), may hold values from -0.125 to 0.125
- w_down: bfloat16 [8, 1024, 2048], P('sp', 'tp'), may hold values from -0.1875 to 0.1875
Outputs:
- layer_out: bfloat16 [4096, 2048], P(('grp', 'sp', 'tp')), parts along dimension 0
There are 2 independent parts, one for each index of `grp`. A program takes and returns all parts, laid end to end along the dimension named above; an argument that names none is the same for every part. Nothing has to cross between parts.
Inputs may be any that keep to these rules, and one draw needn't show every extreme that they name: `routes`: the two numbers of a row differ and lie in the same group of 2 consecutive experts. In each aligned block of 128 rows every expert is named exactly 32 times.
All inputs are finite; a program needn't handle non-finite values.
Results may differ from a plain program's by a relative error of at most 0.0085.
Values may be sent and summed in bfloat16 or wider, within the bound.
A program may use at most 64 MiB of HBM per device.

v0:
```python
import jax
import jax.numpy as jnp
from jax import lax
from jax.sharding import PartitionSpec as P


def shifted(block, axis, distance):
    devices = range(lax.axis_size(axis))
    route = [(i - distance, i) for i in devices if i - distance in devices]
    return lax.ppermute(block, axis, route)


def on_device(
    conv_input,
    pre_gate,
    post_gate,
    conv_taps,
    out_proj,
    residual_in,
    norm_gain,
    routes,
    route_weight,
    w_gate,
    w_up,
    w_down,
):
    shards = lax.axis_size("tp")
    place = lax.axis_index("tp")
    seq_ranks = lax.axis_size("sp")
    channels = conv_input.shape[1]
    width = residual_in.shape[1]
    taps = lax.dynamic_slice_in_dim(conv_taps, place * channels, channels, 1)
    prior_input, prior_gate = shifted((conv_input[-2:], pre_gate[-2:]), "sp", 1)
    gated = jnp.concatenate(
        [
            prior_gate.astype(jnp.float32) * prior_input.astype(jnp.float32),
            pre_gate.astype(jnp.float32) * conv_input.astype(jnp.float32),
        ],
        axis=0,
    )
    conv = gated[2:] * taps[2] + gated[1:-1] * taps[1] + gated[:-2] * taps[0]
    mixed = (post_gate.astype(jnp.float32) * conv).astype(jnp.bfloat16)
    token_rows = lax.all_to_all(mixed, "tp", split_axis=0, concat_axis=1, tiled=True)
    projected = jnp.dot(token_rows, out_proj, preferred_element_type=jnp.float32)
    stream = residual_in.astype(jnp.float32) + projected
    scale = lax.rsqrt(jnp.mean(stream * stream, axis=-1, keepdims=True) + 1e-06)
    normed = (stream * scale * norm_gain).astype(jnp.bfloat16)
    block_rows = routes.shape[0]
    local_experts = w_gate.shape[0]
    experts = local_experts * seq_ranks
    capacity = 2 * block_rows // experts
    flat_routes = routes.reshape(-1)
    position = jnp.arange(flat_routes.shape[0], dtype=jnp.int32)
    earlier = (flat_routes[:, None] == flat_routes[None, :]) & (
        position[None, :] < position[:, None]
    )
    rank = jnp.sum(earlier.astype(jnp.int32), axis=1)
    slot = flat_routes * capacity + rank
    outgoing = (
        jnp.zeros((experts * capacity, width), jnp.bfloat16).at[slot].set(normed[position // 2])
    )
    outgoing = outgoing.reshape(seq_ranks, local_experts, capacity, width)
    spread = lax.all_gather(
        lax.all_to_all(outgoing, "sp", split_axis=0, concat_axis=0, tiled=True)[:, None],
        "tp",
        axis=1,
        tiled=True,
    )
    count = spread.shape[3]
    partials = []
    for expert in range(local_experts):
        rows = spread[:, :, expert].reshape(seq_ranks * shards * count, width)
        gate = jnp.dot(rows, w_gate[expert], preferred_element_type=jnp.float32)
        upper = jnp.dot(rows, w_up[expert], preferred_element_type=jnp.float32)
        hidden = (jax.nn.silu(gate) * upper).astype(jnp.bfloat16)
        part = jnp.dot(hidden, w_down[expert], preferred_element_type=jnp.float32).astype(
            jnp.bfloat16
        )
        partials.append(part.reshape(seq_ranks, shards, count, width))
    stacked = jnp.stack(partials, axis=2)
    summed = lax.psum_scatter(stacked, "tp", scatter_dimension=1, tiled=True).astype(jnp.float32)
    returned = lax.all_to_all(
        summed[:, 0].astype(jnp.bfloat16), "sp", split_axis=0, concat_axis=0, tiled=True
    )
    results = returned.reshape(experts * capacity, width)[slot]
    results = results.reshape(block_rows, 2, width).astype(jnp.float32)
    weighted = jnp.sum(route_weight[:, :, None] * results, axis=1)
    return (stream + weighted).astype(jnp.bfloat16)


def solution(mesh):
    return jax.shard_map(
        on_device,
        mesh=mesh,
        in_specs=(
            P(("grp", "sp"), "tp"),
            P(("grp", "sp"), "tp"),
            P(("grp", "sp"), "tp"),
            P(),
            P(),
            P(("grp", "sp", "tp"), None),
            P(),
            P(("grp", "sp", "tp"), None),
            P(("grp", "sp", "tp"), None),
            P("sp", None, "tp"),
            P("sp", None, "tp"),
            P("sp", "tp", None),
        ),
        out_specs=P(("grp", "sp", "tp"), None),
        check_vma=False,
    )
```

profile of v0, /device:TPU:0, one launch (start us, length us, event | category | flops | bytes accessed | tf_op | source)
XLA Modules:
  0.0 258.8 jit_solution(13987586749709506822)
XLA Ops:
  7.3 4.9 %collective-permute-start = (bf16[2,256]{1,0:T(2,128)(2,1)S(1)}, bf16[2,256]{1,0:T(2,128)(2,1)S(1)}, u32[]{:S(2)}, u32[]{:S(2)}) collective-permute-start(bf16[2,256]{1,0:T(2,128)(2,1)S(1)} %slice.46), channel_id=1, source_target_pairs={{0,4},{4,8},{8,12},{1,5},{5,9},{9,13},{2,6},{6,10},{10,14},{3,7},{... | collective-permute-start | bytes 3080 | tf_op jit(solution)/shard_map/ppermute | solution.py:10
  12.9 3.5 %collective-permute-start.1 = (bf16[2,256]{1,0:T(2,128)(2,1)S(1)}, bf16[2,256]{1,0:T(2,128)(2,1)S(1)}, u32[]{:S(2)}, u32[]{:S(2)}) collective-permute-start(bf16[2,256]{1,0:T(2,128)(2,1)S(1)} %slice.47), channel_id=1, source_target_pairs={{0,4},{4,8},{8,12},{1,5},{5,9},{9,13},{2,6},{6,10},{10,14},{3,7},{... | collective-permute-start | bytes 3080 | tf_op jit(solution)/shard_map/ppermute | solution.py:10
  16.4 1.1 convert_multiply_fusion
  20.5 1.9 fusion.27
  22.4 3.4 %all-to-all-start = ((bf16[4,128,256]{2,1,0:T(8,128)(2,1)}), bf16[4,128,256]{2,1,0:T(8,128)(2,1)S(1)}, u32[]{:S(2)}, u32[]{:S(2)}) async-start(bf16[4,128,256]{2,1,0:T(8,128)(2,1)} %bitcast.3), calls=%async_computation | async-start | bytes 524288 | tf_op jit(solution)/shard_map/all_to_all | solution.py:43
  25.8 5.9 %all-to-all-done = bf16[4,128,256]{2,1,0:T(8,128)(2,1)S(1)} async-done(((bf16[4,128,256]{2,1,0:T(8,128)(2,1)}), bf16[4,128,256]{2,1,0:T(8,128)(2,1)S(1)}, u32[]{:S(2)}, u32[]{:S(2)}) %all-to-all-start) | async-done | bytes 262176 | tf_op jit(solution)/shard_map/all_to_all | solution.py:43
  31.9 3.0 %multiply_reduce_fusion.1 = (f32[128]{0:T(128)S(1)}, f32[128,2048]{1,0:T(8,128)S(1)}) fusion(bf16[128,1024]{0,1:T(8,128)(2,1)S(1)} %bitcast.62, bf16[1024,2048]{1,0:T(8,128)(2,1)} %param.16, bf16[128,2048]{1,0:T(8,128)(2,1)S(1)} %copy-done.1), kind=kOutput, calls=%fused_computation.31 | convolution fusion | flops 537919360 | bytes 6029824 | tf_op jit(solution)/shard_map/dot_general | solution.py:44
  35.1 5.7 %scatter_custom_fusion = bf16[256,2048]{1,0:T(8,128)(2,1)S(1)} fusion(s32[256]{0:T(256)S(1)} %bitcast.67, bf16[128,2048]{1,0:T(8,128)(2,1)S(1)} %multiply_convert_fusion, s32[1024]{0:T(1024)S(1)} %pad_clamp_fusion.1, bf16[]{:T(256)} %constant.35.clone.1), kind=kCustom, calls=%fused_computation.21 | custom fusion | bytes 1048578 | tf_op jit(solution)/shard_map/scatter | solution.py:60
  40.8 28.9 %all_to_all.29 = bf16[4,2,32,2048]{3,2,1,0:T(8,128)(2,1)} all-to-all(bf16[4,2,32,2048]{3,2,1,0:T(8,128)(2,1)S(1)} %bitcast.55), channel_id=1, replica_groups=mesh['grp'=2,'sp'=4,'tp'=4] {'sp'}, dimensions={0} | all-to-all | bytes 2097152 | tf_op jit(solution)/shard_map/all_to_all | solution.py:64
  70.0 32.8 %all-gather.3.cloned.1.call-done = bf16[4,8,32,2048]{3,2,1,0:T(8,128)(2,1)} async-done(((bf16[4,2,32,2048]{3,2,1,0:T(8,128)(2,1)}), bf16[4,8,32,2048]{3,2,1,0:T(8,128)(2,1)}) %all-gather.3.cloned.1.call-update) | async-done | bytes 4194320 | tf_op jit(solution)/shard_map/all_gather | solution.py:63
  102.7 2.8 %fusion.45 = (bf16[4,4,1,32,2048]{4,3,2,1,0:T(8,128)(2,1)S(1)}, bf16[4,4,1,32,2048]{4,3,2,1,0:T(8,128)(2,1)S(1)}) fusion(bf16[4,4,2,32,2048]{4,3,2,1,0:T(8,128)(2,1)} %bitcast.54), kind=kLoop, calls=%fused_computation.73 | loop fusion | bytes 8388608 | tf_op jit(solution)/shard_map/slice | solution.py:72
  105.6 1.5 fusion.10
  107.1 1.5 fusion.5
  108.6 6.0 %convolution_convert_fusion.1 = bf16[512,2048]{1,0:T(8,128)(2,1)} fusion(bf16[512,2048]{1,0:T(8,128)(2,1)} %bitcast.59, bf16[2,256,2048]{2,1,0:T(8,128)(2,1)} %param.23, bf16[2,2048,256]{2,1,0:T(8,128)(2,1)} %param.22, f32[512,256]{1,0:T(8,128)} %fusion.10), kind=kOutput, calls=%fused_computation.5 | convolution fusion | flops 1075576832 | bytes 6815744 | tf_op jit(solution)/shard_map/dot_general | solution.py:76
  114.5 5.4 %convolution_convert_fusion = bf16[512,2048]{1,0:T(8,128)(2,1)} fusion(bf16[512,2048]{1,0:T(8,128)(2,1)S(1)} %bitcast.57, bf16[2,256,2048]{2,1,0:T(8,128)(2,1)} %param.23, bf16[2,2048,256]{2,1,0:T(8,128)(2,1)} %param.22, f32[512,256]{1,0:T(8,128)} %fusion.5), kind=kOutput, calls=%fused_computation.4 | convolution fusion | flops 1075576832 | bytes 6815744 | tf_op jit(solution)/shard_map/dot_general | solution.py:76
  119.9 4.5 %pad_maximum_fusion = bf16[4,4,2,32,2048]{4,3,1,0,2:T(8,128)(2,1)} fusion(bf16[4,4,1,32,2048]{4,3,1,0,2:T(8,128)(2,1)} %bitcast.61, bf16[4,4,1,32,2048]{4,3,1,0,2:T(8,128)(2,1)} %bitcast.60), kind=kLoop, calls=%fused_computation.3 | loop fusion | flops 2097152 | bytes 8388608 | tf_op jit(solution)/shard_map/stack | solution.py:80
  125.7 84.4 %all-reduce.3.cloned.1.call-done = bf16[4,4,2,32,2048]{4,3,1,0,2:T(8,128)(2,1)} async-done(((bf16[4,4,2,32,2048]{4,3,1,0,2:T(8,128)(2,1)}), bf16[4,4,2,32,2048]{4,3,1,0,2:T(8,128)(2,1)}) %all-reduce.3.cloned.1.call-update) | async-done | bytes 4194320
  210.1 1.9 dynamic-slice_bitcast_fusion
  212.1 1.0 copy.33
  213.1 4.6 %all-to-all-start.2 = ((bf16[4,2,32,2048]{3,2,1,0:T(8,128)(2,1)}), bf16[4,2,32,2048]{3,2,1,0:T(8,128)(2,1)S(1)}, u32[]{:S(2)}, u32[]{:S(2)}) async-start(bf16[4,2,32,2048]{3,2,1,0:T(8,128)(2,1)} %copy.33), calls=%async_computation.2 | async-start | bytes 2097152 | tf_op jit(solution)/shard_map/all_to_all | solution.py:82
  217.8 25.3 %all-to-all-done.2 = bf16[4,2,32,2048]{3,2,1,0:T(8,128)(2,1)S(1)} async-done(((bf16[4,2,32,2048]{3,2,1,0:T(8,128)(2,1)}), bf16[4,2,32,2048]{3,2,1,0:T(8,128)(2,1)S(1)}, u32[]{:S(2)}, u32[]{:S(2)}) %all-to-all-start.2) | async-done | bytes 1048608 | tf_op jit(solution)/shard_map/all_to_all | solution.py:82
  243.1 2.3 gather_fusion
  245.5 2.4 reshape.99
  247.8 3.2 %multiply_reduce_fusion = f32[128,2048]{1,0:T(8,128)S(1)} fusion(f32[128,2,2048]{2,1,0:T(2,128)S(1)} %reshape.99, f32[128,2]{1,0:T(8,128)S(1)} %copy.30), kind=kLoop, calls=%fused_computation.7 | loop fusion | flops 786432 | bytes 3146752 | tf_op jit(solution)/shard_map/reduce_sum | solution.py:87
  (38 shorter events, 7.4 us)
Async XLA Ops:
  6.5 25.4 %copy-start.1 = (bf16[128,2048]{1,0:T(8,128)(2,1)S(1)}, bf16[128,2048]{1,0:T(8,128)(2,1)}, u32[]{:S(2)}) copy-start(bf16[128,2048]{1,0:T(8,128)(2,1)} %param.17) | copy-start | bytes 1572868
  7.3 13.2 %collective-permute-start = (bf16[2,256]{1,0:T(2,128)(2,1)S(1)}, bf16[2,256]{1,0:T(2,128)(2,1)S(1)}, u32[]{:S(2)}, u32[]{:S(2)}) collective-permute-start(bf16[2,256]{1,0:T(2,128)(2,1)S(1)} %slice.46), channel_id=1, source_target_pairs={{0,4},{4,8},{8,12},{1,5},{5,9},{9,13},{2,6},{6,10},{10,14},{3,7},{... | collective-permute-start | bytes 3080 | tf_op jit(solution)/shard_map/ppermute | solution.py:10
  12.9 7.5 %collective-permute-start.1 = (bf16[2,256]{1,0:T(2,128)(2,1)S(1)}, bf16[2,256]{1,0:T(2,128)(2,1)S(1)}, u32[]{:S(2)}, u32[]{:S(2)}) collective-permute-start(bf16[2,256]{1,0:T(2,128)(2,1)S(1)} %slice.47), channel_id=1, source_target_pairs={{0,4},{4,8},{8,12},{1,5},{5,9},{9,13},{2,6},{6,10},{10,14},{3,7},{... | collective-permute-start | bytes 3080 | tf_op jit(solution)/shard_map/ppermute | solution.py:10
  22.4 9.4 %all-to-all-start = ((bf16[4,128,256]{2,1,0:T(8,128)(2,1)}), bf16[4,128,256]{2,1,0:T(8,128)(2,1)S(1)}, u32[]{:S(2)}, u32[]{:S(2)}) async-start(bf16[4,128,256]{2,1,0:T(8,128)(2,1)} %bitcast.3), calls=%async_computation | async-start | bytes 524288 | tf_op jit(solution)/shard_map/all_to_all | solution.py:43
  25.8 76.9 %all-gather.3.cloned.1.call-start = ((), (), s32[]{:S(2)}) async-start(), calls=%async_computation.3 | async-start | bytes 5242880 | tf_op jit(solution)/shard_map/all_gather | solution.py:63
  31.9 3.0 %copy-start.2 = (f32[2048]{0:T(1024)S(1)}, f32[2048]{0:T(1024)}, u32[]{:S(2)}) copy-start(f32[2048]{0:T(1024)} %param.18) | copy-start | bytes 24580
  69.7 140.4 %all-reduce.3.cloned.1.call-start = ((), (), s32[]{:S(2)}) async-start(), calls=%async_computation.4 | async-start | bytes 8388608
  102.7 2.9 %copy-start.4 = (bf16[2,2048,256]{2,1,0:T(8,128)(2,1)S(1)}, bf16[2,2048,256]{2,1,0:T(8,128)(2,1)}, u32[]{:S(2)}) copy-start(bf16[2,2048,256]{2,1,0:T(8,128)(2,1)} %param.21) | copy-start | bytes 6291460
  105.5 1.6 copy-start
  124.5 0.7 copy-start.5
  212.1 5.6 %copy-start.3 = (f32[128,2]{0,1:T(2,128)S(1)}, f32[128,2]{0,1:T(2,128)}, u32[]{:S(2)}) copy-start(f32[128,2]{0,1:T(2,128)} %param.20) | copy-start | bytes 3076
  213.1 30.0 %all-to-all-start.2 = ((bf16[4,2,32,2048]{3,2,1,0:T(8,128)(2,1)}), bf16[4,2,32,2048]{3,2,1,0:T(8,128)(2,1)S(1)}, u32[]{:S(2)}, u32[]{:S(2)}) async-start(bf16[4,2,32,2048]{3,2,1,0:T(8,128)(2,1)} %copy.33), calls=%async_computation.2 | async-start | bytes 2097152 | tf_op jit(solution)/shard_map/all_to_all | solution.py:82
Sparse Core Ops, SparseCore 0:
  69.8 32.8 all-gather.2
  124.6 85.4 all-reduce.2
where the time goes:
time: 259 us
  waiting for transfers between devices  148 us (57%)
  blocking collectives  28.9 us (11%)
  local copies, waits for them, and re-layouts  21.2 us (8%)
  matrix products  17.4 us (7%)
  starting transfers between devices  16.7 us (6%)
  between operations  13.6 us (5%)
  other arithmetic  12.7 us (5%)
    unnamed x3, waiting for transfers between devices  84.5 us
    all_gather x1, waiting for transfers between devices, on_device(): lax.all_gather(lax.all_to_all(outgoing, 'sp', split_axis=0, concat_axis=0...  32.8 us
    all_to_all x1, blocking collectives, on_device(): lax.all_to_all(outgoing, 'sp', split_axis=0, concat_axis=0, tiled=True)  28.9 us
    all_to_all x1, waiting for transfers between devices, on_device(): lax.all_to_all(summed[:, 0].astype(jnp.bfloat16), 'sp', split_axis=0, con...  25.3 us
    dot_general x2, matrix products, on_device(): jnp.dot(hidden, w_down[expert], preferred_element_type=jnp.float32)  11.3 us
    ppermute x2, starting transfers between devices, shifted(): return lax.ppermute(block, axis, route)  8.42 us
    all_to_all x1, waiting for transfers between devices, on_device(): lax.all_to_all(mixed, 'tp', split_axis=0, concat_axis=1, tiled=True)  5.91 us
    scatter x1, local copies, waits for them, and re-layouts, on_device(): jnp.zeros((experts * capacity, width), jnp.bfloat16).at[slot]  5.7 us
  transfers between devices with their start and end apart: 6, of which 4 were waited for; matrix products, arithmetic and copies ran while one was open for 2% of the time, Pallas kernels for 0%

commit v1 on v0

--- a/solution.py
+++ b/solution.py
@@ -1,7 +1,15 @@
+import functools
+
 import jax
 import jax.numpy as jnp
 from jax import lax
+from jax.experimental import pallas as pl
+from jax.experimental.pallas import tpu as pltpu
 from jax.sharding import PartitionSpec as P
+
+GROUPS = 4
+LANES = 128
+F32, BF16 = jnp.float32, jnp.bfloat16
 
 
 def shifted(block, axis, distance):
@@ -10,7 +18,7 @@
     return lax.ppermute(block, axis, route)
 
 
-def on_device(
+def generic(
     conv_input,
     pre_gate,
     post_gate,
@@ -88,6 +96,372 @@
     return (stream + weighted).astype(jnp.bfloat16)
 
 
+def dot(a, b):
+    return jnp.dot(a, b, preferred_element_type=F32)
+
+
+def fused_kernel(
+    conv_input,
+    pre_gate,
+    post_gate,
+    conv_taps,
+    proj_hbm,
+    residual,
+    gain,
+    routes,
+    route_weight,
+    gate_hbm,
+    up_hbm,
+    down_hbm,
+    out,
+    proj,
+    w_gate,
+    w_up,
+    w_down,
+    halo,
+    gated,
+    mix_out,
+    mix_in,
+    stream,
+    leaving,
+    tok,
+    hidden,
+    part,
+    from_core,
+    kept,
+    to_chip,
+    from_chip,
+    to_home,
+    home,
+    load_sem,
+    halo_send,
+    halo_recv,
+    mix_send,
+    mix_recv,
+    z_send,
+    z_recv,
+    x_send,
+    x_recv,
+    c_send,
+    c_recv,
+    d_send,
+    d_recv,
+    one_send,
+    one_recv,
+    two_send,
+    two_recv,
+    home_send,
+    home_recv,
+):
+    s, t = lax.axis_index("sp"), lax.axis_index("tp")
+    rows, width = residual.shape
+    channels = conv_input.shape[1]
+    cap = rows // GROUPS
+    units = w_gate.shape[2]
+    core, chip, far = t + 1 - 2 * (t % 2), (t + 2) % 4, 3 - t
+    sp_of = [s, s + 1 - 2 * (s % 2), (s + 2) % 4, 3 - s]
+    pos = lambda place: (place % 2) * 2 + place // 2
+    block = lambda place: pl.ds(pl.multiple_of(pos(place) * cap, cap), cap)
+    pending = []
+
+    def send(src, dst, send_sem, recv_sem, **where):
+        copy = pltpu.make_async_remote_copy(
+            src_ref=src,
+            dst_ref=dst,
+            send_sem=send_sem,
+            recv_sem=recv_sem,
+            device_id=where,
+            device_id_type=pl.DeviceIdType.MESH,
+        )
+        copy.start()
+        pending.append(copy)
+        return copy
+
+    loads = []
+    for i, (a, b) in enumerate(
+        ((proj_hbm, proj), (gate_hbm, w_gate), (up_hbm, w_up), (down_hbm, w_down))
+    ):
+        loads.append(pltpu.make_async_copy(a, b, load_sem.at[i]))
+        loads[-1].start()
+
+    barrier = pltpu.get_barrier_semaphore()
+    for other in (core, chip, far):
+        pl.semaphore_signal(
+            barrier, inc=1, device_id={"tp": other}, device_id_type=pl.DeviceIdType.MESH
+        )
+    for other in sp_of[1:]:
+        pl.semaphore_signal(
+            barrier, inc=1, device_id={"sp": other}, device_id_type=pl.DeviceIdType.MESH
+        )
+    pl.semaphore_wait(barrier, 6)
+
+    count = conv_input.shape[0]
+    halo_copies = [
+        send(
+            ref.at[pl.ds(count - 16, 16), :],
+            halo.at[i],
+            halo_send.at[i],
+            halo_recv.at[i],
+            sp=(s + 1) % 4,
+        )
+        for i, ref in enumerate((conv_input, pre_gate))
+    ]
+    gated[pl.ds(8, count), :] = pre_gate[...].astype(F32) * conv_input[...].astype(F32)
+    taps = conv_taps[:, pl.ds(pl.multiple_of(t * channels, channels), channels)]
+    for copy in halo_copies:
+        copy.wait_recv()
+    before = halo[0, 8:16, :].astype(F32) * halo[1, 8:16, :].astype(F32)
+    gated[0:8, :] = jnp.where(s > 0, before, 0.0)
+
+    def mix(place):
+        start = pl.multiple_of(place * rows, rows)
+        g = gated[pl.ds(start, rows + 8), :]
+        conv = g[8:] * taps[2:3] + g[7:-1] * taps[1:2] + g[6:-2] * taps[0:1]
+        return (post_gate[pl.ds(start, rows), :].astype(F32) * conv).astype(BF16)
+
+    mix_copies = []
+    for i, place in enumerate((chip, far, core)):
+        mix_out[i] = mix(place)
+        mix_copies.append(
+            send(mix_out.at[i], mix_in.at[t], mix_send.at[i], mix_recv.at[i], tp=place)
+        )
+    mix_in[t] = mix(t)
+
+    first, second = routes[:, 0:1], routes[:, 1:2]
+    lane = lax.broadcasted_iota(jnp.int32, (rows, LANES), 1)
+    epg = w_gate.shape[0]
+    member = (first >= lane * epg) & (first < lane * epg + epg) & (lane < GROUPS)
+    down = lax.broadcasted_iota(jnp.int32, (rows, rows), 0)
+    across = lax.broadcasted_iota(jnp.int32, (rows, rows), 1)
+    earlier = jnp.where(across < down, 1.0, 0.0).astype(BF16)
+    member = jnp.where(member, 1.0, 0.0)
+    rank = dot(earlier, member.astype(BF16))
+    slot = jnp.sum(member * (rank + (lane * cap).astype(F32)), axis=1, keepdims=True)
+    back = jnp.where(slot == across.astype(F32), 1.0, 0.0)
+    pick = back.T.astype(BF16)
+    back = back.astype(BF16)
+    low = jnp.where(first < second, route_weight[:, 0:1], route_weight[:, 1:2])
+    high = jnp.where(first < second, route_weight[:, 1:2], route_weight[:, 0:1])
+    low_top, high_top = low.astype(BF16).astype(F32), high.astype(BF16).astype(F32)
+    scales = jnp.where(
+        lane == 0,
+        low_top,
+        jnp.where(
+            lane == 1,
+            low - low_top,
+            jnp.where(lane == 2, high_top, jnp.where(lane == 3, high - high_top, 0.0)),
+        ),
+    ).astype(BF16)
+    leaving[:, pl.ds(width, LANES)] = dot(pick, scales).astype(BF16)
+
+    loads[0].wait()
+    for copy in mix_copies:
+        copy.wait_recv()
+    tile = 512
+
+    def project(n, squares):
+        cols = pl.ds(pl.multiple_of(n * tile, tile), tile)
+        total = residual[:, cols].astype(F32)
+        for j in range(4):
+            total += dot(mix_in[j], proj[pl.ds(j * channels, channels), cols])
+        stream[:, cols] = total
+        return squares + jnp.sum(total * total, axis=1, keepdims=True)
+
+    squares = lax.fori_loop(0, width // tile, project, jnp.zeros((rows, 1), F32))
+    scale = lax.rsqrt(squares / width + 1e-06)
+
+    def norm(n, carry):
+        cols = pl.ds(pl.multiple_of(n * tile, tile), tile)
+        row = (stream[:, cols] * scale * gain[:, cols]).astype(BF16)
+        leaving[:, cols] = dot(pick, row).astype(BF16)
+        return carry
+
+    lax.fori_loop(0, width // tile, norm, 0)
+
+    group_rows = lambda g: pl.ds(pl.multiple_of(g * cap, cap), cap)
+    z_copies = [None]
+    for k in (1, 2, 3):
+        g = sp_of[k]
+        z_copies.append(
+            send(
+                leaving.at[group_rows(g), :],
+                tok.at[s, block(t), :],
+                z_send.at[k],
+                z_recv.at[k],
+                sp=g,
+            )
+        )
+    x_copies, c_copies, d_copies = [], [], []
+
+    def forward(k):
+        src = leaving.at[group_rows(s), :]
+        if k:
+            z_copies[k].wait_recv()
+            src = tok.at[sp_of[k], block(t), :]
+        dst = tok.at[sp_of[k], block(t), :]
+        x_copies.append(send(src, dst, x_send.at[k], x_recv.at[k], tp=chip))
+        c_copies.append(send(src, dst, c_send.at[k], c_recv.at[k], tp=core))
+
+    forward(0)
+    tok[s, block(t), :] = leaving[group_rows(s), :]
+    for load in loads[1:]:
+        load.wait()
+
+    def compute(k):
+        g = sp_of[k]
+        x = tok[g, :, 0:width]
+        for e in range(epg):
+            w = tok[g, :, pl.ds(width, LANES)].astype(F32)
+            w = w[:, 2 * e : 2 * e + 1] + w[:, 2 * e + 1 : 2 * e + 2]
+            gate = dot(x, w_gate[e])
+            upper = dot(x, w_up[e])
+            act = gate / (1.0 + jnp.exp(-gate)) * upper * w
+            hidden[:, pl.ds(e * units, units)] = act.astype(BF16)
+
+        def lower(n, carry):
+            cols = pl.ds(pl.multiple_of(n * tile, tile), tile)
+            part[k, :, cols] = dot(hidden[...], w_down[:, cols]).astype(BF16)
+            return carry
+
+        lax.fori_loop(0, width // tile, lower, 0)
+
+    half = 2 * cap
+    core_rows = lambda c: pl.ds(pl.multiple_of(c * half, half), half)
+    one_copies, two_copies, home_copies = [], [], []
+
+    def stage_one(k):
+        one_copies.append(
+            send(
+                part.at[k, core_rows(1 - t % 2), :],
+                from_core.at[k],
+                one_send.at[k],
+                one_recv.at[k],
+                tp=core,
+            )
+        )
+
+    def stage_two(k):
+        one_copies[k].wait_recv()
+        for mine in (False, True):
+            x = t // 2 if mine else 1 - t // 2
+            base = pl.multiple_of((t % 2) * half + x * cap, cap)
+            near = pl.multiple_of(x * cap, cap)
+            total = part[k, pl.ds(base, cap), :].astype(F32)
+            total += from_core[k, pl.ds(near, cap), :].astype(F32)
+            if mine:
+                kept[k] = total
+            else:
+                to_chip[k] = total.astype(BF16)
+                two_copies.append(
+                    send(to_chip.at[k], from_chip.at[k], two_send.at[k], two_recv.at[k], tp=chip)
+                )
+
+    def stage_three(k):
+        two_copies[k].wait_recv()
+        total = (kept[k] + from_chip[k].astype(F32)).astype(BF16)
+        if k == 0:
+            home[group_rows(s), :] = total
+            home_copies.append(None)
+        else:
+            to_home[k] = total
+            home_copies.append(
+                send(
+                    to_home.at[k],
+                    home.at[group_rows(s), :],
+                    home_send.at[k],
+                    home_recv.at[k],
+                    sp=sp_of[k],
+                )
+            )
+
+    for k in range(4):
+        if k + 1 < 4:
+            forward(k + 1)
+        x_copies[k].wait_recv()
+        arrived = tok.at[sp_of[k], block(chip), :]
+        d_copies.append(send(arrived, arrived, d_send.at[k], d_recv.at[k], tp=core))
+        if k >= 1:
+            stage_two(k - 1)
+        c_copies[k].wait_recv()
+        d_copies[k].wait_recv()
+        compute(k)
+        stage_one(k)
+        if k >= 2:
+            stage_three(k - 2)
+    stage_two(3)
+    stage_three(2)
+    stage_three(3)
+    for copy in home_copies[1:]:
+        copy.wait_recv()
+
+    def finish(n, carry):
+        cols = pl.ds(pl.multiple_of(n * tile, tile), tile)
+        out[:, cols] = (stream[:, cols] + dot(back, home[:, cols])).astype(BF16)
+        return carry
+
+    lax.fori_loop(0, width // tile, finish, 0)
+    for copy in pending:
+        copy.wait_send()
+
+
+def fused(*args):
+    (conv_input, _, _, _, out_proj, residual, gain, _, _, w_gate, w_up, w_down) = args
+    rows, width = residual.shape
+    count, channels = conv_input.shape
+    local, _, units = w_gate.shape
+    cap = rows // GROUPS
+    w_down = w_down.reshape(local * units, width)
+    args = args[:6] + (gain.reshape(1, width),) + args[7:11] + (w_down,)
+    vmem = pl.BlockSpec(memory_space=pltpu.VMEM)
+    far = pl.BlockSpec(memory_space=pl.ANY)
+    sems = pltpu.SemaphoreType.DMA
+    return pl.pallas_call(
+        fused_kernel,
+        out_shape=jax.ShapeDtypeStruct((rows, width), BF16),
+        in_specs=[vmem] * 4 + [far] + [vmem] * 4 + [far] * 3,
+        out_specs=vmem,
+        scratch_shapes=[
+            pltpu.VMEM(out_proj.shape, BF16),
+            pltpu.VMEM(w_gate.shape, BF16),
+            pltpu.VMEM(w_up.shape, BF16),
+            pltpu.VMEM(w_down.shape, BF16),
+            pltpu.VMEM((2, 16, channels), BF16),
+            pltpu.VMEM((count + 8, channels), F32),
+            pltpu.VMEM((3, rows, channels), BF16),
+            pltpu.VMEM((4, rows, channels), BF16),
+            pltpu.VMEM((rows, width), F32),
+            pltpu.VMEM((rows, width + LANES), BF16),
+            pltpu.VMEM((4, 4 * cap, width + LANES), BF16),
+            pltpu.VMEM((4 * cap, local * units), BF16),
+            pltpu.VMEM((4, 4 * cap, width), BF16),
+            pltpu.VMEM((4, 2 * cap, width), BF16),
+            pltpu.VMEM((4, cap, width), F32),
+            pltpu.VMEM((4, cap, width), BF16),
+            pltpu.VMEM((4, cap, width), BF16),
+            pltpu.VMEM((4, cap, width), BF16),
+            pltpu.VMEM((rows, width), BF16),
+            sems((4,)),
+            sems((2,)),
+            sems((2,)),
+            sems((3,)),
+            sems((3,)),
+        ]
+        + [sems((4,))] * 14,
+        compiler_params=pltpu.CompilerParams(
+            collective_id=0, has_side_effects=True, vmem_limit_bytes=56 << 20
+        ),
+    )(*args)
+
+
+def on_device(*args):
+    residual, routes, w_gate = args[5], args[7], args[9]
+    rows, local, seq_ranks = residual.shape[0], w_gate.shape[0], lax.axis_size("sp")
+    dense = local == routes.shape[1] == 2 and local * seq_ranks == local * GROUPS
+    if dense and lax.axis_size("tp") == 4 and rows % LANES == 0:
+        return fused(*args)
+    return generic(*args)
+
+
 def solution(mesh):
     return jax.shard_map(
         on_device,

time: 259 us -> 58.5 us (0.23)
  waiting for transfers between devices: 148 us -> 0 us
  Pallas kernels: 0 us -> 53.6 us
  blocking collectives: 28.9 us -> 0 us
  matrix products: 17.4 us -> 0 us
  starting transfers between devices: 16.7 us -> 0 us
  local copies, waits for them, and re-layouts: 21.2 us -> 4.7 us
  between operations: 13.6 us -> 0.01 us
  other arithmetic: 12.7 us -> 0 us
    unnamed x3 -> x0, waiting for transfers between devices: 84.5 us -> none
    pallas_call x0 -> x1, Pallas kernels: none -> 53.6 us  [fused(): pl.pallas_call(fused_kernel, out_shape=jax.ShapeDtypeStruct((rows, width)...]
    all_gather x1 -> x0, waiting for transfers between devices: 32.8 us -> none  [on_device(): lax.all_gather(lax.all_to_all(outgoing, 'sp', split_axis=0, concat_axis=0...]
    all_to_all x2 -> x0, waiting for transfers between devices: 31.2 us -> none  [the longest x1 25.3 us: on_device(): lax.all_to_all(summed[:, 0].astype(jnp.bfloat16), 'sp', split_axis=0, con...]
    all_to_all x1 -> x0, blocking collectives: 28.9 us -> none  [on_device(): lax.all_to_all(outgoing, 'sp', split_axis=0, concat_axis=0, tiled=True)]
    dot_general x5 -> x0, matrix products: 17.4 us -> none  [the longest x2 11.3 us: on_device(): jnp.dot(hidden, w_down[expert], preferred_element_type=jnp.float32)]
    ppermute x2 -> x0, starting transfers between devices: 8.42 us -> none  [shifted(): return lax.ppermute(block, axis, route)]
    all_to_all x2 -> x0, starting transfers between devices: 8.01 us -> none  [the longest x1 4.6 us: on_device(): lax.all_to_all(summed[:, 0].astype(jnp.bfloat16), 'sp', split_axis=0, con...]
  transfers between devices with their start and end apart: 6 -> 0, of which waited for: 4 -> 0; matrix products, arithmetic and copies ran while one was open for 2% -> 0% of each run, Pallas kernels for 0% -> 0%
where the time goes in v1:
time: 58.5 us; the launch traced here: 58.3 us
  Pallas kernels  53.6 us (92%)
  local copies, waits for them, and re-layouts  4.7 us (8%)
    pallas_call x1, Pallas kernels, fused(): pl.pallas_call(fused_kernel, out_shape=jax.ShapeDtypeStruct((rows, width)...  53.6 us
    unnamed x3, local copies, waits for them, and re-layouts  4.7 us

profile of v1, /device:TPU:0, one launch (start us, length us, event | category | flops | bytes accessed | tf_op | source)
XLA Modules:
  0.0 58.3 jit_solution(16941838930136197194)
XLA Ops:
  0.0 1.4 %copy.13.routes = s32[128,2]{1,0:T(8,128)} copy(s32[128,2]{0,1:T(2,128)} %param.19) | data formatting | bytes 2048 | tf_op args[7]
  1.4 1.4 %copy.14.route_weight = f32[128,2]{1,0:T(8,128)} copy(f32[128,2]{0,1:T(2,128)} %param.20) | data formatting | bytes 2048 | tf_op args[8]
  2.8 53.6 %shard_map.118 = bf16[128,2048]{1,0:T(8,128)(2,1)} custom-call(bf16[512,256]{1,0:T(8,128)(2,1)} %conv_input.1, bf16[512,256]{1,0:T(8,128)(2,1)} %pre_gate.1, bf16[512,256]{1,0:T(8,128)(2,1)} %post_gate.1, f32[3,1024]{1,0:T(4,128)} %conv_taps.1, bf16[1024,2048]{1,0:T(8,128)(2,1)} %proj_hbm.1, bf16[128,2048]{1,0:T(8,128)(2,1)} %residual.1, f32[1,2048]{1,0:T(1,128)} %bitcast.3, ...), custom_call_target="tpu_custom_call" | custom-call | tf_op jit(solution)/shard_map/pallas_call | solution.py:418
  56.4 1.9 %copy.16 = bf16[128,2048]{1,0:T(8,128)(2,1)} copy(bf16[128,2048]{1,0:T(8,128)(2,1)} %shard_map.118) | data formatting | bytes 1048576

commit v2 on v1

--- a/solution.py
+++ b/solution.py
@@ -101,12 +101,12 @@
 
 
 def fused_kernel(
-    conv_input,
-    pre_gate,
-    post_gate,
+    input_hbm,
+    pre_hbm,
+    post_hbm,
     conv_taps,
     proj_hbm,
-    residual,
+    residual_hbm,
     gain,
     routes,
     route_weight,
@@ -114,6 +114,10 @@
     up_hbm,
     down_hbm,
     out,
+    conv_input,
+    pre_gate,
+    post_gate,
+    residual,
     proj,
     w_gate,
     w_up,
@@ -177,13 +181,6 @@
         pending.append(copy)
         return copy
 
-    loads = []
-    for i, (a, b) in enumerate(
-        ((proj_hbm, proj), (gate_hbm, w_gate), (up_hbm, w_up), (down_hbm, w_down))
-    ):
-        loads.append(pltpu.make_async_copy(a, b, load_sem.at[i]))
-        loads[-1].start()
-
     barrier = pltpu.get_barrier_semaphore()
     for other in (core, chip, far):
         pl.semaphore_signal(
@@ -193,6 +190,55 @@
         pl.semaphore_signal(
             barrier, inc=1, device_id={"sp": other}, device_id_type=pl.DeviceIdType.MESH
         )
+    loads = []
+    for i, (a, b) in enumerate(
+        (
+            (input_hbm, conv_input),
+            (pre_hbm, pre_gate),
+            (post_hbm, post_gate),
+            (residual_hbm, residual),
+            (proj_hbm, proj),
+            (gate_hbm, w_gate),
+            (up_hbm, w_up),
+            (down_hbm, w_down),
+        )
+    ):
+        loads.append(pltpu.make_async_copy(a, b, load_sem.at[i]))
+        loads[-1].start()
+
+    first, second = routes[0:1, :], routes[1:2, :]
+    epg = w_gate.shape[0]
+    down = lax.broadcasted_iota(jnp.int32, (rows, rows), 0)
+    across = lax.broadcasted_iota(jnp.int32, (rows, rows), 1)
+    group = lax.broadcasted_iota(jnp.int32, (16, rows), 0)
+    member = (first >= group * epg) & (first < group * epg + epg) & (group < GROUPS)
+    member = jnp.where(member, 1.0, 0.0)
+    earlier = jnp.where(down < across, 1.0, 0.0).astype(BF16)
+    rank = dot(member.astype(BF16), earlier)
+    slot = jnp.sum(member * (rank + (group * cap).astype(F32)), axis=0, keepdims=True)
+    pick = jnp.where(slot == down.astype(F32), 1.0, 0.0)
+    back = pick.T.astype(BF16)
+    pick = pick.astype(BF16)
+    low = jnp.where(first < second, route_weight[0:1, :], route_weight[1:2, :])
+    high = jnp.where(first < second, route_weight[1:2, :], route_weight[0:1, :])
+    low_top, high_top = low.astype(BF16).astype(F32), high.astype(BF16).astype(F32)
+    line = lax.broadcasted_iota(jnp.int32, (LANES, rows), 0)
+    scales = jnp.where(
+        line == 0,
+        low_top,
+        jnp.where(
+            line == 1,
+            low - low_top,
+            jnp.where(line == 2, high_top, jnp.where(line == 3, high - high_top, 0.0)),
+        ),
+    ).astype(BF16)
+    scales = lax.dot_general(
+        pick, scales, (((1,), (1,)), ((), ())), preferred_element_type=F32
+    )
+    leaving[:, pl.ds(width, LANES)] = scales.astype(BF16)
+
+    loads[0].wait()
+    loads[1].wait()
     pl.semaphore_wait(barrier, 6)
 
     count = conv_input.shape[0]
@@ -208,10 +254,7 @@
     ]
     gated[pl.ds(8, count), :] = pre_gate[...].astype(F32) * conv_input[...].astype(F32)
     taps = conv_taps[:, pl.ds(pl.multiple_of(t * channels, channels), channels)]
-    for copy in halo_copies:
-        copy.wait_recv()
-    before = halo[0, 8:16, :].astype(F32) * halo[1, 8:16, :].astype(F32)
-    gated[0:8, :] = jnp.where(s > 0, before, 0.0)
+    loads[2].wait()
 
     def mix(place):
         start = pl.multiple_of(place * rows, rows)
@@ -219,96 +262,111 @@
         conv = g[8:] * taps[2:3] + g[7:-1] * taps[1:2] + g[6:-2] * taps[0:1]
         return (post_gate[pl.ds(start, rows), :].astype(F32) * conv).astype(BF16)
 
-    mix_copies = []
-    for i, place in enumerate((chip, far, core)):
+    def send_mixed(i, place):
         mix_out[i] = mix(place)
-        mix_copies.append(
-            send(mix_out.at[i], mix_in.at[t], mix_send.at[i], mix_recv.at[i], tp=place)
-        )
+        send(mix_out.at[i], mix_in.at[t], mix_send.at[i], mix_recv.at[t], tp=place)
+
+    def wait_mixed(place):
+        pltpu.make_async_remote_copy(
+            src_ref=mix_in.at[place],
+            dst_ref=mix_in.at[place],
+            send_sem=mix_send.at[0],
+            recv_sem=mix_recv.at[place],
+            device_id={"tp": place},
+            device_id_type=pl.DeviceIdType.MESH,
+        ).wait_recv()
+
+    across_chip = 2 * (1 - t // 2)
+    send_mixed(0, across_chip + 1)
+    for copy in halo_copies:
+        copy.wait_recv()
+    before = halo[0, 8:16, :].astype(F32) * halo[1, 8:16, :].astype(F32)
+    gated[0:8, :] = jnp.where(s > 0, before, 0.0)
+    send_mixed(1, across_chip)
+    send_mixed(2, core)
     mix_in[t] = mix(t)
 
-    first, second = routes[:, 0:1], routes[:, 1:2]
-    lane = lax.broadcasted_iota(jnp.int32, (rows, LANES), 1)
-    epg = w_gate.shape[0]
-    member = (first >= lane * epg) & (first < lane * epg + epg) & (lane < GROUPS)
-    down = lax.broadcasted_iota(jnp.int32, (rows, rows), 0)
-    across = lax.broadcasted_iota(jnp.int32, (rows, rows), 1)
-    earlier = jnp.where(across < down, 1.0, 0.0).astype(BF16)
-    member = jnp.where(member, 1.0, 0.0)
-    rank = dot(earlier, member.astype(BF16))
-    slot = jnp.sum(member * (rank + (lane * cap).astype(F32)), axis=1, keepdims=True)
-    back = jnp.where(slot == across.astype(F32), 1.0, 0.0)
-    pick = back.T.astype(BF16)
-    back = back.astype(BF16)
-    low = jnp.where(first < second, route_weight[:, 0:1], route_weight[:, 1:2])
-    high = jnp.where(first < second, route_weight[:, 1:2], route_weight[:, 0:1])
-    low_top, high_top = low.astype(BF16).astype(F32), high.astype(BF16).astype(F32)
-    scales = jnp.where(
-        lane == 0,
-        low_top,
-        jnp.where(
-            lane == 1,
-            low - low_top,
-            jnp.where(lane == 2, high_top, jnp.where(lane == 3, high - high_top, 0.0)),
-        ),
-    ).astype(BF16)
-    leaving[:, pl.ds(width, LANES)] = dot(pick, scales).astype(BF16)
-
-    loads[0].wait()
-    for copy in mix_copies:
-        copy.wait_recv()
     tile = 512
-
-    def project(n, squares):
-        cols = pl.ds(pl.multiple_of(n * tile, tile), tile)
+    tiles = width // tile
+    column = lambda n: pl.ds(pl.multiple_of(n * tile, tile), tile)
+    weights_of = lambda place: pl.ds(pl.multiple_of(place * channels, channels), channels)
+    loads[3].wait()
+    loads[4].wait()
+    wait_mixed(core)
+
+    def project_near(n, carry):
+        cols = column(n)
         total = residual[:, cols].astype(F32)
-        for j in range(4):
-            total += dot(mix_in[j], proj[pl.ds(j * channels, channels), cols])
+        for place in (t, core):
+            total += dot(mix_in[place], proj[weights_of(place), cols])
+        stream[:, cols] = total
+        return carry
+
+    lax.fori_loop(0, tiles, project_near, 0)
+    wait_mixed(chip)
+    wait_mixed(far)
+
+    def project_far(n, squares):
+        cols = column(n)
+        total = stream[:, cols]
+        for place in (chip, far):
+            total += dot(mix_in[place], proj[weights_of(place), cols])
         stream[:, cols] = total
         return squares + jnp.sum(total * total, axis=1, keepdims=True)
 
-    squares = lax.fori_loop(0, width // tile, project, jnp.zeros((rows, 1), F32))
+    squares = lax.fori_loop(0, tiles, project_far, jnp.zeros((rows, 1), F32))
     scale = lax.rsqrt(squares / width + 1e-06)
 
     def norm(n, carry):
-        cols = pl.ds(pl.multiple_of(n * tile, tile), tile)
+        cols = column(n)
         row = (stream[:, cols] * scale * gain[:, cols]).astype(BF16)
         leaving[:, cols] = dot(pick, row).astype(BF16)
         return carry
 
-    lax.fori_loop(0, width // tile, norm, 0)
-
+    split = width // 2
+    halves = (pl.ds(0, split), pl.ds(split, split))
+    sent = (pl.ds(0, split), pl.ds(split, split + LANES))
     group_rows = lambda g: pl.ds(pl.multiple_of(g * cap, cap), cap)
-    z_copies = [None]
-    for k in (1, 2, 3):
+    z_copies, x_copies, c_copies, d_copies = {}, {}, {}, {}
+    one_copies, two_copies, home_copies = {}, {}, {}
+
+    def forward(k, h):
+        src = leaving.at[group_rows(s), sent[h]]
+        if k:
+            z_copies[k, h].wait_recv()
+            src = tok.at[sp_of[k], block(t), sent[h]]
+        dst = tok.at[sp_of[k], block(t), sent[h]]
+        i = 2 * k + h
+        x_copies[k, h] = send(src, dst, x_send.at[i], x_recv.at[i], tp=chip)
+        c_copies[k, h] = send(src, dst, c_send.at[i], c_recv.at[i], tp=core)
+
+    def pass_on(k, h):
+        x_copies[k, h].wait_recv()
+        i = 2 * k + h
+        arrived = tok.at[sp_of[k], block(chip), sent[h]]
+        d_copies[k, h] = send(arrived, arrived, d_send.at[i], d_recv.at[i], tp=core)
+
+    for h in (0, 1):
+        lax.fori_loop(h * tiles // 2, (h + 1) * tiles // 2, norm, 0)
+        for k in (1, 2, 3):
+            i = 2 * k + h
+            z_copies[k, h] = send(
+                leaving.at[group_rows(sp_of[k]), sent[h]],
+                tok.at[s, block(t), sent[h]],
+                z_send.at[i],
+                z_recv.at[i],
+                sp=sp_of[k],
+            )
+        forward(0, h)
+    tok[s, block(t), :] = leaving[group_rows(s), :]
+    for load in loads[5:]:
+        load.wait()
+
+    def raise_units(k):
         g = sp_of[k]
-        z_copies.append(
-            send(
-                leaving.at[group_rows(g), :],
-                tok.at[s, block(t), :],
-                z_send.at[k],
-                z_recv.at[k],
-                sp=g,
-            )
-        )
-    x_copies, c_copies, d_copies = [], [], []
-
-    def forward(k):
-        src = leaving.at[group_rows(s), :]
-        if k:
-            z_copies[k].wait_recv()
-            src = tok.at[sp_of[k], block(t), :]
-        dst = tok.at[sp_of[k], block(t), :]
-        x_copies.append(send(src, dst, x_send.at[k], x_recv.at[k], tp=chip))
-        c_copies.append(send(src, dst, c_send.at[k], c_recv.at[k], tp=core))
-
-    forward(0)
-    tok[s, block(t), :] = leaving[group_rows(s), :]
-    for load in loads[1:]:
-        load.wait()
-
-    def compute(k):
-        g = sp_of[k]
+        for h in (0, 1):
+            c_copies[k, h].wait_recv()
+            d_copies[k, h].wait_recv()
         x = tok[g, :, 0:width]
         for e in range(epg):
             w = tok[g, :, pl.ds(width, LANES)].astype(F32)
@@ -318,88 +376,103 @@
             act = gate / (1.0 + jnp.exp(-gate)) * upper * w
             hidden[:, pl.ds(e * units, units)] = act.astype(BF16)
 
+    both = 2 * cap
+    core_rows = lambda c: pl.ds(pl.multiple_of(c * both, both), both)
+
+    def lower_units(k, h):
         def lower(n, carry):
-            cols = pl.ds(pl.multiple_of(n * tile, tile), tile)
+            cols = column(n)
             part[k, :, cols] = dot(hidden[...], w_down[:, cols]).astype(BF16)
             return carry
 
-        lax.fori_loop(0, width // tile, lower, 0)
-
-    half = 2 * cap
-    core_rows = lambda c: pl.ds(pl.multiple_of(c * half, half), half)
-    one_copies, two_copies, home_copies = [], [], []
-
-    def stage_one(k):
-        one_copies.append(
-            send(
-                part.at[k, core_rows(1 - t % 2), :],
-                from_core.at[k],
-                one_send.at[k],
-                one_recv.at[k],
-                tp=core,
-            )
-        )
-
-    def stage_two(k):
-        one_copies[k].wait_recv()
+        lax.fori_loop(h * tiles // 2, (h + 1) * tiles // 2, lower, 0)
+        i = 2 * k + h
+        one_copies[k, h] = send(
+            part.at[k, core_rows(1 - t % 2), halves[h]],
+            from_core.at[k, :, halves[h]],
+            one_send.at[i],
+            one_recv.at[i],
+            tp=core,
+        )
+
+    def add_core(k, h):
+        one_copies[k, h].wait_recv()
+        cols, i = halves[h], 2 * k + h
         for mine in (False, True):
             x = t // 2 if mine else 1 - t // 2
-            base = pl.multiple_of((t % 2) * half + x * cap, cap)
+            base = pl.multiple_of((t % 2) * both + x * cap, cap)
             near = pl.multiple_of(x * cap, cap)
-            total = part[k, pl.ds(base, cap), :].astype(F32)
-            total += from_core[k, pl.ds(near, cap), :].astype(F32)
+            total = part[k, pl.ds(base, cap), cols].astype(F32)
+            total += from_core[k, pl.ds(near, cap), cols].astype(F32)
             if mine:
-                kept[k] = total
+                kept[k, :, cols] = total
             else:
-                to_chip[k] = total.astype(BF16)
-                two_copies.append(
-                    send(to_chip.at[k], from_chip.at[k], two_send.at[k], two_recv.at[k], tp=chip)
+                to_chip[k, :, cols] = total.astype(BF16)
+                two_copies[k, h] = send(
+                    to_chip.at[k, :, cols],
+                    from_chip.at[k, :, cols],
+                    two_send.at[i],
+                    two_recv.at[i],
+                    tp=chip,
                 )
 
-    def stage_three(k):
-        two_copies[k].wait_recv()
-        total = (kept[k] + from_chip[k].astype(F32)).astype(BF16)
+    def add_chip(k, h):
+        two_copies[k, h].wait_recv()
+        cols, i = halves[h], 2 * k + h
+        total = (kept[k, :, cols] + from_chip[k, :, cols].astype(F32)).astype(BF16)
         if k == 0:
-            home[group_rows(s), :] = total
-            home_copies.append(None)
+            home[group_rows(s), cols] = total
         else:
-            to_home[k] = total
-            home_copies.append(
-                send(
-                    to_home.at[k],
-                    home.at[group_rows(s), :],
-                    home_send.at[k],
-                    home_recv.at[k],
-                    sp=sp_of[k],
-                )
+            to_home[k, :, cols] = total
+            home_copies[k, h] = send(
+                to_home.at[k, :, cols],
+                home.at[group_rows(s), cols],
+                home_send.at[i],
+                home_recv.at[i],
+                sp=sp_of[k],
             )
 
-    for k in range(4):
-        if k + 1 < 4:
-            forward(k + 1)
-        x_copies[k].wait_recv()
-        arrived = tok.at[sp_of[k], block(chip), :]
-        d_copies.append(send(arrived, arrived, d_send.at[k], d_recv.at[k], tp=core))
-        if k >= 1:
-            stage_two(k - 1)
-        c_copies[k].wait_recv()
-        d_copies[k].wait_recv()
-        compute(k)
-        stage_one(k)
-        if k >= 2:
-            stage_three(k - 2)
-    stage_two(3)
-    stage_three(2)
-    stage_three(3)
-    for copy in home_copies[1:]:
-        copy.wait_recv()
+    def halved(stage, k):
+        stage(k, 0)
+        stage(k, 1)
+
+    def step(k):
+        raise_units(k)
+        halved(lower_units, k)
+
+    for h in (0, 1):
+        forward(1, h)
+        pass_on(0, h)
+    step(0)
+    for h in (0, 1):
+        forward(2, h)
+        pass_on(1, h)
+    step(1)
+    for h in (0, 1):
+        forward(3, h)
+        pass_on(2, h)
+    halved(add_core, 1)
+    step(2)
+    halved(pass_on, 3)
+    halved(add_core, 2)
+    halved(add_core, 0)
+    halved(add_chip, 1)
+    step(3)
+    for h in (0, 1):
+        add_core(3, h)
+    halved(add_chip, 2)
+    halved(add_chip, 0)
+    halved(add_chip, 3)
 
     def finish(n, carry):
-        cols = pl.ds(pl.multiple_of(n * tile, tile), tile)
+        cols = column(n)
         out[:, cols] = (stream[:, cols] + dot(back, home[:, cols])).astype(BF16)
         return carry
 
-    lax.fori_loop(0, width // tile, finish, 0)
+    for h in (0, 1):
+        for k in (1, 2, 3):
+            home_copies[k, h].wait_recv()
+        lax.fori_loop(h * tiles // 2, (h + 1) * tiles // 2, finish, 0)
     for copy in pending:
         copy.wait_send()
 
@@ -411,16 +484,20 @@
     local, _, units = w_gate.shape
     cap = rows // GROUPS
     w_down = w_down.reshape(local * units, width)
-    args = args[:6] + (gain.reshape(1, width),) + args[7:11] + (w_down,)
+    args = args[:6] + (gain.reshape(1, width), args[7].T, args[8].T) + args[9:11] + (w_down,)
     vmem = pl.BlockSpec(memory_space=pltpu.VMEM)
     far = pl.BlockSpec(memory_space=pl.ANY)
     sems = pltpu.SemaphoreType.DMA
     return pl.pallas_call(
         fused_kernel,
         out_shape=jax.ShapeDtypeStruct((rows, width), BF16),
-        in_specs=[vmem] * 4 + [far] + [vmem] * 4 + [far] * 3,
+        in_specs=[far] * 3 + [vmem] + [far] * 2 + [vmem] * 3 + [far] * 3,
         out_specs=vmem,
         scratch_shapes=[
+            pltpu.VMEM((count, channels), BF16),
+            pltpu.VMEM((count, channels), BF16),
+            pltpu.VMEM((count, channels), BF16),
+            pltpu.VMEM((rows, width), BF16),
             pltpu.VMEM(out_proj.shape, BF16),
             pltpu.VMEM(w_gate.shape, BF16),
             pltpu.VMEM(w_up.shape, BF16),
@@ -440,13 +517,13 @@
             pltpu.VMEM((4, cap, width), BF16),
             pltpu.VMEM((4, cap, width), BF16),
             pltpu.VMEM((rows, width), BF16),
-            sems((4,)),
+            sems((8,)),
             sems((2,)),
             sems((2,)),
             sems((3,)),
-            sems((3,)),
+            sems((4,)),
         ]
-        + [sems((4,))] * 14,
+        + [sems((8,))] * 14,
         compiler_params=pltpu.CompilerParams(
             collective_id=0, has_side_effects=True, vmem_limit_bytes=56 << 20
         ),

time: 58.5 us -> 54.4 us (0.930); the launches traced: 58.3 us -> 53.5 us
  local copies, waits for them, and re-layouts: 4.7 us -> 1.88 us
  Pallas kernels: 53.6 us -> 51.6 us
    unnamed x3 -> x1, local copies, waits for them, and re-layouts: 4.7 us -> 1.88 us
    pallas_call x1, Pallas kernels: 53.6 us -> 51.6 us  [fused(): pl.pallas_call(fused_kernel, out_shape=jax.ShapeDtypeStruct((rows, width)...]
where the time goes in v2:
time: 54.4 us; the launch traced here: 53.5 us
  Pallas kernels  51.6 us (95%)
  local copies, waits for them, and re-layouts  1.88 us (3%)
    pallas_call x1, Pallas kernels, fused(): pl.pallas_call(fused_kernel, out_shape=jax.ShapeDtypeStruct((rows, width)...  51.6 us
    unnamed x1, local copies, waits for them, and re-layouts  1.88 us

profile of v2, /device:TPU:0, one launch (start us, length us, event | category | flops | bytes accessed | tf_op | source)
XLA Modules:
  0.0 53.5 jit_solution(6633175173499010721)
XLA Ops:
  0.0 51.6 %shard_map.118 = bf16[128,2048]{1,0:T(8,128)(2,1)} custom-call(bf16[512,256]{1,0:T(8,128)(2,1)} %input_hbm.1, bf16[512,256]{1,0:T(8,128)(2,1)} %pre_hbm.1, bf16[512,256]{1,0:T(8,128)(2,1)} %post_hbm.1, f32[3,1024]{1,0:T(4,128)} %conv_taps.1, bf16[1024,2048]{1,0:T(8,128)(2,1)} %proj_hbm.1, bf16[128,2048]{1,0:T(8,128)(2,1)} %residual_hbm.1, ...), custom_call_target="tpu_custom_call" | custom-call | tf_op jit(solution)/shard_map/pallas_call | solution.py:491
  51.6 1.9 %copy.14 = bf16[128,2048]{1,0:T(8,128)(2,1)} copy(bf16[128,2048]{1,0:T(8,128)(2,1)} %shard_map.118) | data formatting | bytes 1048576

commit v3 on v2

--- a/solution.py
+++ b/solution.py
@@ -165,7 +165,6 @@
     core, chip, far = t + 1 - 2 * (t % 2), (t + 2) % 4, 3 - t
     sp_of = [s, s + 1 - 2 * (s % 2), (s + 2) % 4, 3 - s]
     pos = lambda place: (place % 2) * 2 + place // 2
-    block = lambda place: pl.ds(pl.multiple_of(pos(place) * cap, cap), cap)
     pending = []
 
     def send(src, dst, send_sem, recv_sem, **where):
@@ -323,19 +322,21 @@
         leaving[:, cols] = dot(pick, row).astype(BF16)
         return carry
 
-    split = width // 2
-    halves = (pl.ds(0, split), pl.ds(split, split))
-    sent = (pl.ds(0, split), pl.ds(split, split + LANES))
+    lax.fori_loop(0, tiles, norm, 0)
+
+    some = cap // 2
     group_rows = lambda g: pl.ds(pl.multiple_of(g * cap, cap), cap)
+    part_rows = lambda g, h: pl.ds(pl.multiple_of(g * cap + h * some, some), some)
+    block = lambda place: pl.ds(pl.multiple_of(pos(place) * some, some), some)
     z_copies, x_copies, c_copies, d_copies = {}, {}, {}, {}
     one_copies, two_copies, home_copies = {}, {}, {}
 
     def forward(k, h):
-        src = leaving.at[group_rows(s), sent[h]]
+        src = leaving.at[part_rows(s, h), :]
         if k:
             z_copies[k, h].wait_recv()
-            src = tok.at[sp_of[k], block(t), sent[h]]
-        dst = tok.at[sp_of[k], block(t), sent[h]]
+            src = tok.at[sp_of[k], h, block(t), :]
+        dst = tok.at[sp_of[k], h, block(t), :]
         i = 2 * k + h
         x_copies[k, h] = send(src, dst, x_send.at[i], x_recv.at[i], tp=chip)
         c_copies[k, h] = send(src, dst, c_send.at[i], c_recv.at[i], tp=core)
@@ -343,74 +344,75 @@
     def pass_on(k, h):
         x_copies[k, h].wait_recv()
         i = 2 * k + h
-        arrived = tok.at[sp_of[k], block(chip), sent[h]]
+        arrived = tok.at[sp_of[k], h, block(chip), :]
         d_copies[k, h] = send(arrived, arrived, d_send.at[i], d_recv.at[i], tp=core)
 
+    for k, h in ((1, 0), (1, 1), (2, 0), (2, 1), (3, 0), (3, 1)):
+        i = 2 * k + h
+        z_copies[k, h] = send(
+            leaving.at[part_rows(sp_of[k], h), :],
+            tok.at[s, h, block(t), :],
+            z_send.at[i],
+            z_recv.at[i],
+            sp=sp_of[k],
+        )
     for h in (0, 1):
-        lax.fori_loop(h * tiles // 2, (h + 1) * tiles // 2, norm, 0)
-        for k in (1, 2, 3):
-            i = 2 * k + h
-            z_copies[k, h] = send(
-                leaving.at[group_rows(sp_of[k]), sent[h]],
-                tok.at[s, block(t), sent[h]],
-                z_send.at[i],
-                z_recv.at[i],
-                sp=sp_of[k],
-            )
         forward(0, h)
-    tok[s, block(t), :] = leaving[group_rows(s), :]
+        tok[s, h, block(t), :] = leaving[part_rows(s, h), :]
     for load in loads[5:]:
         load.wait()
 
-    def raise_units(k):
-        g = sp_of[k]
-        for h in (0, 1):
+    def experts(k, *one):
+        own = one or (0, 1)
+        for h in own:
             c_copies[k, h].wait_recv()
             d_copies[k, h].wait_recv()
-        x = tok[g, :, 0:width]
+        g, low_half, m = sp_of[k], own[0], len(own)
+        where, length = pl.ds(low_half, m), m * 2 * cap
+        x = tok[g, where, :, 0:width].reshape(length, width)
+        top = tok[g, where, :, pl.ds(width, LANES)].reshape(length, LANES).astype(F32)
         for e in range(epg):
-            w = tok[g, :, pl.ds(width, LANES)].astype(F32)
-            w = w[:, 2 * e : 2 * e + 1] + w[:, 2 * e + 1 : 2 * e + 2]
+            w = top[:, 2 * e : 2 * e + 1] + top[:, 2 * e + 1 : 2 * e + 2]
             gate = dot(x, w_gate[e])
             upper = dot(x, w_up[e])
             act = gate / (1.0 + jnp.exp(-gate)) * upper * w
-            hidden[:, pl.ds(e * units, units)] = act.astype(BF16)
-
-    both = 2 * cap
-    core_rows = lambda c: pl.ds(pl.multiple_of(c * both, both), both)
-
-    def lower_units(k, h):
+            hidden[0:length, pl.ds(e * units, units)] = act.astype(BF16)
+
         def lower(n, carry):
             cols = column(n)
-            part[k, :, cols] = dot(hidden[...], w_down[:, cols]).astype(BF16)
+            rows_out = dot(hidden[0:length, :], w_down[:, cols]).astype(BF16)
+            part[k, where, :, cols] = rows_out.reshape(m, 2 * cap, tile)
             return carry
 
-        lax.fori_loop(h * tiles // 2, (h + 1) * tiles // 2, lower, 0)
-        i = 2 * k + h
-        one_copies[k, h] = send(
-            part.at[k, core_rows(1 - t % 2), halves[h]],
-            from_core.at[k, :, halves[h]],
-            one_send.at[i],
-            one_recv.at[i],
-            tp=core,
-        )
+        lax.fori_loop(0, tiles, lower, 0)
+        for h in own:
+            i = 2 * k + h
+            one_copies[k, h] = send(
+                part.at[k, h, core_rows(1 - t % 2), :],
+                from_core.at[k, h],
+                one_send.at[i],
+                one_recv.at[i],
+                tp=core,
+            )
+
+    core_rows = lambda c: pl.ds(pl.multiple_of(c * cap, cap), cap)
 
     def add_core(k, h):
         one_copies[k, h].wait_recv()
-        cols, i = halves[h], 2 * k + h
+        i = 2 * k + h
         for mine in (False, True):
             x = t // 2 if mine else 1 - t // 2
-            base = pl.multiple_of((t % 2) * both + x * cap, cap)
-            near = pl.multiple_of(x * cap, cap)
-            total = part[k, pl.ds(base, cap), cols].astype(F32)
-            total += from_core[k, pl.ds(near, cap), cols].astype(F32)
+            base = pl.multiple_of((t % 2) * cap + x * some, some)
+            near = pl.multiple_of(x * some, some)
+            total = part[k, h, pl.ds(base, some), :].astype(F32)
+            total += from_core[k, h, pl.ds(near, some), :].astype(F32)
             if mine:
-                kept[k, :, cols] = total
+                kept[k, h] = total
             else:
-                to_chip[k, :, cols] = total.astype(BF16)
+                to_chip[k, h] = total.astype(BF16)
                 two_copies[k, h] = send(
-                    to_chip.at[k, :, cols],
-                    from_chip.at[k, :, cols],
+                    to_chip.at[k, h],
+                    from_chip.at[k, h],
                     two_send.at[i],
                     two_recv.at[i],
                     tp=chip,
@@ -418,61 +420,44 @@
 
     def add_chip(k, h):
         two_copies[k, h].wait_recv()
-        cols, i = halves[h], 2 * k + h
-        total = (kept[k, :, cols] + from_chip[k, :, cols].astype(F32)).astype(BF16)
+        i = 2 * k + h
+        total = (kept[k, h] + from_chip[k, h].astype(F32)).astype(BF16)
         if k == 0:
-            home[group_rows(s), cols] = total
+            home[part_rows(s, h), :] = total
         else:
-            to_home[k, :, cols] = total
+            to_home[k, h] = total
             home_copies[k, h] = send(
-                to_home.at[k, :, cols],
-                home.at[group_rows(s), cols],
+                to_home.at[k, h],
+                home.at[part_rows(s, h), :],
                 home_send.at[i],
                 home_recv.at[i],
                 sp=sp_of[k],
             )
 
-    def halved(stage, k):
-        stage(k, 0)
-        stage(k, 1)
-
-    def step(k):
-        raise_units(k)
-        halved(lower_units, k)
-
-    for h in (0, 1):
-        forward(1, h)
-        pass_on(0, h)
-    step(0)
-    for h in (0, 1):
-        forward(2, h)
-        pass_on(1, h)
-    step(1)
-    for h in (0, 1):
-        forward(3, h)
-        pass_on(2, h)
-    halved(add_core, 1)
-    step(2)
-    halved(pass_on, 3)
-    halved(add_core, 2)
-    halved(add_core, 0)
-    halved(add_chip, 1)
-    step(3)
-    for h in (0, 1):
-        add_core(3, h)
-    halved(add_chip, 2)
-    halved(add_chip, 0)
-    halved(add_chip, 3)
+    stages = dict(F=forward, P=pass_on, C=experts, A=add_core, B=add_chip)
+    order = (
+        "F10 P00 F11 P01",
+        "C0 F20 P10 F21",
+        "P11 C1 F30 P20",
+        "F31 P21 A10 A11",
+        "C2 P30 P31 A20",
+        "A21 B10 B11 C3",
+        "A30 A31 B20 B21",
+        "A00 A01 B30 B31",
+        "B00 B01",
+    )
+    for line_of in order:
+        for stage in line_of.split():
+            stages[stage[0]](*map(int, stage[1:]))
 
     def finish(n, carry):
         cols = column(n)
         out[:, cols] = (stream[:, cols] + dot(back, home[:, cols])).astype(BF16)
         return carry
 
-    for h in (0, 1):
-        for k in (1, 2, 3):
-            home_copies[k, h].wait_recv()
-        lax.fori_loop(h * tiles // 2, (h + 1) * tiles // 2, finish, 0)
+    for copy in home_copies.values():
+        copy.wait_recv()
+    lax.fori_loop(0, tiles, finish, 0)
     for copy in pending:
         copy.wait_send()
 
@@ -508,14 +493,14 @@
             pltpu.VMEM((4, rows, channels), BF16),
             pltpu.VMEM((rows, width), F32),
             pltpu.VMEM((rows, width + LANES), BF16),
-            pltpu.VMEM((4, 4 * cap, width + LANES), BF16),
+            pltpu.VMEM((4, 2, 2 * cap, width + LANES), BF16),
             pltpu.VMEM((4 * cap, local * units), BF16),
-            pltpu.VMEM((4, 4 * cap, width), BF16),
-            pltpu.VMEM((4, 2 * cap, width), BF16),
-            pltpu.VMEM((4, cap, width), F32),
-            pltpu.VMEM((4, cap, width), BF16),
-            pltpu.VMEM((4, cap, width), BF16),
-            pltpu.VMEM((4, cap, width), BF16),
+            pltpu.VMEM((4, 2, 2 * cap, width), BF16),
+            pltpu.VMEM((4, 2, cap, width), BF16),
+            pltpu.VMEM((4, 2, cap // 2, width), F32),
+            pltpu.VMEM((4, 2, cap // 2, width), BF16),
+            pltpu.VMEM((4, 2, cap // 2, width), BF16),
+            pltpu.VMEM((4, 2, cap // 2, width), BF16),
             pltpu.VMEM((rows, width), BF16),
             sems((8,)),
             sems((2,)),

time: 54.4 us -> 53.3 us (0.980); the launches traced: 53.5 us -> 53 us
  no operation moved by 1% of the time
where the time goes in v3:
time: 53.3 us; the launch traced here: 53 us
  Pallas kernels  51.1 us (96%)
  local copies, waits for them, and re-layouts  1.88 us (4%)
    pallas_call x1, Pallas kernels, fused(): pl.pallas_call(fused_kernel, out_shape=jax.ShapeDtypeStruct((rows, width)...  51.1 us
    unnamed x1, local copies, waits for them, and re-layouts  1.88 us

profile of v3, /device:TPU:0, one launch (start us, length us, event | category | flops | bytes accessed | tf_op | source)
XLA Modules:
  0.0 53.0 jit_solution(18071964644717555575)
XLA Ops:
  0.0 51.1 %shard_map.118 = bf16[128,2048]{1,0:T(8,128)(2,1)} custom-call(bf16[512,256]{1,0:T(8,128)(2,1)} %input_hbm.1, bf16[512,256]{1,0:T(8,128)(2,1)} %pre_hbm.1, bf16[512,256]{1,0:T(8,128)(2,1)} %post_hbm.1, f32[3,1024]{1,0:T(4,128)} %conv_taps.1, bf16[1024,2048]{1,0:T(8,128)(2,1)} %proj_hbm.1, bf16[128,2048]{1,0:T(8,128)(2,1)} %residual_hbm.1, ...), custom_call_target="tpu_custom_call" | custom-call | tf_op jit(solution)/shard_map/pallas_call | solution.py:476
  51.1 1.9 %copy.14 = bf16[128,2048]{1,0:T(8,128)(2,1)} copy(bf16[128,2048]{1,0:T(8,128)(2,1)} %shard_map.118) | data formatting | bytes 1048576
